TPU v7x, 32 devices: a whole 2x2x4 slice. The times are simulated.
32 devices in a mesh: rep: 2 (over x), fs: 4 (over z), tp: 4 (over y, core).
Axes of the slice: x: 2, y: 2, z: 4, core: 2. Of those that a mesh axis runs over, the one named last changes fastest.
Arguments:
- tokens: bfloat16 [4096, 2048], P(('rep', 'fs', 'tp')), may hold values from -6 to 6
- mix_gain: bfloat16 [2048], replicated, may hold values from 0.099609375 to 1.8984375
- gate_proj: bfloat16 [2048, 512], P('fs', 'tp'), may hold values from -0.125 to 0.125
- value_proj: bfloat16 [2048, 512], P('fs', 'tp'), may hold values from -1 to 1
- layer_gain: bfloat16 [512], replicated, may hold values from 0.099609375 to 1.8984375
- layer_shift: bfloat16 [512], replicated, may hold values from -3 to 3
- mix_kernel: bfloat16 [4, 128, 128], replicated, may hold values from -0.5 to 0.5
- mix_offset: bfloat16 [4, 128], replicated, may hold values from -4 to 4
- out_proj: bfloat16 [2048, 512], P('fs', 'tp'), may hold values from -0.25 to 0.25
- ffn_gain: bfloat16 [2048], replicated, may hold values from 0.099609375 to 1.8984375
- ffn_gate: bfloat16 [2048, 5632], P('fs', 'tp'), may hold values from -0.125 to 0.125
- ffn_up: bfloat16 [2048, 5632], P('fs', 'tp'), may hold values from -0.125 to 0.125
- ffn_down: bfloat16 [2048, 5632], P('fs', 'tp'), may hold values from -0.078125 to 0.078125
Outputs:
- layer_out: bfloat16 [4096, 2048], P(('rep', 'fs', 'tp'))
All inputs are finite; a program needn't handle non-finite values.
Results may differ from a plain program's by a relative error of at most 0.015.
Values may be sent and summed in bfloat16 or wider, within the bound.
A program may use at most 64 MiB of HBM per device.

v0:
```python
import jax
import jax.numpy as jnp
from jax import lax
from jax.sharding import PartitionSpec as P

epsilon = 1e-06


def rms_norm(rows, gain):
    floats = rows.astype(jnp.float32)
    scale = lax.rsqrt(jnp.mean(floats * floats, axis=-1, keepdims=True) + epsilon)
    return (floats * scale * gain.astype(jnp.float32)).astype(jnp.bfloat16)


def contract_last(left, right):
    return lax.dot_general(
        left, right, (((1,), (1,)), ((), ())), preferred_element_type=jnp.float32
    )


def per_device(
    tokens,
    mix_gain,
    gate_proj,
    value_proj,
    layer_gain,
    layer_shift,
    mix_kernel,
    mix_offset,
    out_proj,
    ffn_gain,
    ffn_gate,
    ffn_up,
    ffn_down,
):
    normed = rms_norm(tokens, mix_gain)
    gate_rows, value_rows, out_rows = (
        lax.all_gather(gate_proj, "fs", axis=0, tiled=True),
        lax.all_gather(value_proj, "fs", axis=0, tiled=True),
        lax.all_gather(out_proj, "fs", axis=0, tiled=True),
    )
    mix_width = layer_gain.shape[0]
    groups = mix_kernel.shape[0]
    span_len = mix_kernel.shape[1]
    causal = jnp.tril(jnp.ones((span_len, span_len), dtype=bool))
    masked = jnp.where(causal[None], mix_kernel, jnp.zeros_like(mix_kernel))
    local_width = gate_rows.shape[1]
    first_col = lax.axis_index("tp") * local_width
    joined = jnp.concatenate([gate_rows, value_rows], axis=1)
    preact = jnp.dot(
        lax.all_gather(normed, "tp", axis=0, tiled=True), joined, preferred_element_type=jnp.float32
    )
    gate_u = jax.nn.gelu(preact[:, :local_width])
    activated = jax.nn.gelu(preact[:, local_width:])
    row_sum, squares = lax.psum(
        (jnp.sum(activated, axis=-1), jnp.sum(activated * activated, axis=-1)), "tp"
    )
    center = (row_sum / mix_width)[:, None]
    spread = (squares / mix_width)[:, None] - center * center
    gain_part = lax.dynamic_slice_in_dim(layer_gain, first_col, local_width).astype(jnp.float32)
    shift_part = lax.dynamic_slice_in_dim(layer_shift, first_col, local_width).astype(jnp.float32)
    values = ((activated - center) * lax.rsqrt(spread + epsilon) * gain_part + shift_part).astype(
        jnp.bfloat16
    )
    group_id = first_col // (mix_width // groups)
    kernel = lax.dynamic_index_in_dim(masked, group_id, 0, keepdims=False)
    offset = lax.dynamic_index_in_dim(mix_offset, group_id, 0, keepdims=False).astype(jnp.float32)
    mixing = jnp.einsum(
        "ts,nsc->ntc",
        kernel,
        values.reshape(-1, span_len, local_width),
        preferred_element_type=jnp.float32,
    )
    mixing = mixing + offset[None, :, None]
    gated_rows = (gate_u * mixing.reshape(gate_u.shape)).astype(jnp.bfloat16)
    mixer_out = lax.psum_scatter(
        contract_last(gated_rows, out_rows).astype(jnp.bfloat16),
        "tp",
        scatter_dimension=0,
        tiled=True,
    ).astype(jnp.float32)
    middle = (tokens.astype(jnp.float32) + mixer_out).astype(jnp.bfloat16)
    normed2 = rms_norm(middle, ffn_gain)
    gathered = lax.all_gather(normed2, "tp", axis=0, tiled=True)
    gate_pre = jnp.dot(
        gathered,
        lax.all_gather(ffn_gate, "fs", axis=0, tiled=True),
        preferred_element_type=jnp.float32,
    )
    up_pre = jnp.dot(
        gathered,
        lax.all_gather(ffn_up, "fs", axis=0, tiled=True),
        preferred_element_type=jnp.float32,
    )
    hidden = (jax.nn.silu(gate_pre) * up_pre).astype(jnp.bfloat16)
    partial_value = contract_last(hidden, lax.all_gather(ffn_down, "fs", axis=0, tiled=True))
    summed = lax.psum_scatter(
        partial_value.astype(jnp.bfloat16), "tp", scatter_dimension=0, tiled=True
    ).astype(jnp.float32)
    return (middle.astype(jnp.float32) + summed).astype(jnp.bfloat16)


def solution(mesh):
    placed = (
        P(("rep", "fs", "tp"), None),
        P(),
        P("fs", "tp"),
        P("fs", "tp"),
        P(),
        P(),
        P(),
        P(),
        P("fs", "tp"),
        P(),
        P("fs", "tp"),
        P("fs", "tp"),
        P("fs", "tp"),
    )
    return jax.shard_map(
        per_device,
        mesh=mesh,
        in_specs=placed,
        out_specs=P(("rep", "fs", "tp"), None),
        check_vma=False,
    )
```

profile of v0, /device:TPU:0, one launch (start us, length us, event | category | flops | bytes accessed | tf_op | source)
XLA Modules:
  0.0 472.7 jit_solution(3375747574779029369)
XLA Ops:
  7.4 0.7 convert_element_type.64
  8.1 1.2 fusion.1
  9.3 2.0 fusion.3
  11.4 0.0 reduce-scatter.3.cloned.1.call-start
  11.5 0.7 bitcast_convert_fusion
  12.2 0.8 dynamic-slice_convert_fusion
  12.9 17.6 %all_gather.25 = bf16[2048,128]{1,0:T(8,128)(2,1)S(1)} all-gather(bf16[512,128]{1,0:T(8,128)(2,1)} %param.15), channel_id=1, replica_groups=mesh['rep'=2,'fs'=4,'tp'=4] {'fs'}, dimensions={0}, use_global_device_ids=true | all-gather | bytes 655360 | tf_op jit(solution)/shard_map/all_gather | solution.py:38
  30.5 16.7 %all_gather.26 = bf16[2048,128]{1,0:T(8,128)(2,1)S(1)} all-gather(bf16[512,128]{1,0:T(8,128)(2,1)S(1)} %copy-done.2), channel_id=1, replica_groups=mesh['rep'=2,'fs'=4,'tp'=4] {'fs'}, dimensions={0}, use_global_device_ids=true | all-gather | bytes 655360 | tf_op jit(solution)/shard_map/all_gather | solution.py:39
  47.2 15.6 %all_gather.27 = bf16[2048,128]{1,0:T(8,128)(2,1)S(1)} all-gather(bf16[512,128]{1,0:T(8,128)(2,1)S(1)} %copy-done.3), channel_id=1, replica_groups=mesh['rep'=2,'fs'=4,'tp'=4] {'fs'}, dimensions={0}, use_global_device_ids=true | all-gather | bytes 655360 | tf_op jit(solution)/shard_map/all_gather | solution.py:40
  62.8 2.3 fusion.9
  65.2 0.2 fusion.37
  65.4 5.7 %all-reduce = (f32[512]{0:T(512)S(1)}, f32[512]{0:T(512)S(1)}) all-reduce(f32[512]{0:T(512)S(1)} %get-tuple-element.6, f32[512]{0:T(512)S(1)} %get-tuple-element.5), channel_id=1, replica_groups=mesh['rep'=2,'fs'=4,'tp'=4] {'tp'}, use_global_device_ids=true, to_apply=%region_4.5 | all-reduce | flops 1024 | bytes 8192 | tf_op jit(solution)/shard_map/psum | solution.py:55
  71.1 0.2 add_convert_fusion
  71.3 0.9 convolution_add_fusion
  72.2 0.1 fusion.21
  72.4 2.1 convolution_convert_fusion
  74.5 0.0 all-gather.10.cloned.1.call-start
  74.5 0.5 all-gather.10.cloned.1.call-update
  75.1 31.4 %reduce-scatter.3.cloned.1.call-done = bf16[128,2048]{1,0:T(8,128)(2,1)} async-done(((bf16[512,2048]{1,0:T(8,128)(2,1)}), bf16[128,2048]{1,0:T(8,128)(2,1)}) %reduce-scatter.3.cloned.1.call-update) | async-done | bytes 524304 | tf_op jit(solution)/shard_map/reduce_scatter | solution.py:76
  106.5 1.3 fusion.5
  107.8 2.0 fusion.7
  109.9 0.0 all-gather.12.cloned.1.call-start
  110.0 0.5 all-gather.12.cloned.1.call-update
  110.6 0.7 all-gather.14.cloned.1.call-update
  111.3 72.6 %all-gather.10.cloned.1.call-done = bf16[2048,1408]{1,0:T(8,128)(2,1)} async-done(((bf16[512,1408]{1,0:T(8,128)(2,1)}), bf16[2048,1408]{1,0:T(8,128)(2,1)}) %all-gather.10.cloned.1.call-update) | async-done | bytes 5767184 | tf_op jit(solution)/shard_map/all_gather | solution.py:87
  183.9 22.1 %all-gather.8.cloned.1.call-done = bf16[512,2048]{1,0:T(8,128)(2,1)} async-done(((bf16[128,2048]{1,0:T(8,128)(2,1)}), bf16[512,2048]{1,0:T(8,128)(2,1)}) %all-gather.8.cloned.1.call-update) | async-done | bytes 2097168 | tf_op jit(solution)/shard_map/all_gather | solution.py:84
  206.0 8.4 %fusion.38 = f32[512,1408]{1,0:T(8,128)} fusion(bf16[512,2048]{1,0:T(8,128)(2,1)} %all-gather.8.cloned.1.call-done, bf16[2048,1408]{1,0:T(8,128)(2,1)} %all-gather.10.cloned.1.call-done), kind=kOutput, calls=%fused_computation.60 | convolution fusion | flops 2952790016 | bytes 10747904 | tf_op jit(solution)/shard_map/dot_general | solution.py:85
  214.4 99.6 %all-gather.12.cloned.1.call-done = bf16[2048,1408]{1,0:T(8,128)(2,1)} async-done(((bf16[512,1408]{1,0:T(8,128)(2,1)}), bf16[2048,1408]{1,0:T(8,128)(2,1)}) %all-gather.12.cloned.1.call-update) | async-done | bytes 5767184 | tf_op jit(solution)/shard_map/all_gather | solution.py:92
  314.0 106.4 %all-gather.14.cloned.1.call-done = bf16[2048,1408]{1,0:T(8,128)(2,1)} async-done(((bf16[512,1408]{1,0:T(8,128)(2,1)}), bf16[2048,1408]{1,0:T(8,128)(2,1)}) %all-gather.14.cloned.1.call-update) | async-done | bytes 5767184 | tf_op jit(solution)/shard_map/all_gather | solution.py:96
  420.5 13.2 %convolution_convert_fusion.1 = bf16[512,2048]{1,0:T(8,128)(2,1)} fusion(bf16[2048,1408]{1,0:T(8,128)(2,1)} %all-gather.14.cloned.1.call-done, bf16[512,2048]{1,0:T(8,128)(2,1)S(1)} %copy-done.5, bf16[2048,1408]{1,0:T(8,128)(2,1)} %all-gather.12.cloned.1.call-done, f32[512,1408]{1,0:T(8,128)} %fusion.38), kind=kOutput, calls=%fused_computation.3 | convolution fusion | flops 5910953984 | bytes 18612224 | tf_op jit(solution)/shard_map/dot_general | solution.py:16
  433.7 29.6 %reduce-scatter.5.cloned.1.call-done = bf16[128,2048]{1,0:T(8,128)(2,1)} async-done(((bf16[512,2048]{1,0:T(8,128)(2,1)}), bf16[128,2048]{1,0:T(8,128)(2,1)}) %reduce-scatter.5.cloned.1.call-update) | async-done | bytes 524304 | tf_op jit(solution)/shard_map/reduce_scatter | solution.py:97
  463.3 2.1 fusion.8
  (26 shorter events, 0.3 us)
Async XLA Ops:
  7.4 23.2 %copy-start.2 = (bf16[512,128]{1,0:T(8,128)(2,1)S(1)}, bf16[512,128]{1,0:T(8,128)(2,1)}, u32[]{:S(2)}) copy-start(bf16[512,128]{1,0:T(8,128)(2,1)} %param.16) | copy-start | bytes 393220
  7.4 39.9 %copy-start.3 = (bf16[512,128]{1,0:T(8,128)(2,1)S(1)}, bf16[512,128]{1,0:T(8,128)(2,1)}, u32[]{:S(2)}) copy-start(bf16[512,128]{1,0:T(8,128)(2,1)} %param.21) | copy-start | bytes 393220
  7.4 55.5 %all-gather.6.cloned.1.call-start = ((), (), s32[]{:S(2)}) async-start(), calls=%async_computation.2 | async-start | bytes 2621440 | tf_op jit(solution)/shard_map/all_gather | solution.py:51
  11.4 95.1 %reduce-scatter.3.cloned.1.call-start = ((), (), s32[]{:S(2)}) async-start(), calls=%async_computation.3 | async-start | bytes 2621440 | tf_op jit(solution)/shard_map/reduce_scatter | solution.py:76
  72.3 2.7 copy-start.4
  72.4 34.2 %copy-start = (bf16[128,2048]{1,0:T(8,128)(2,1)S(1)}, bf16[128,2048]{1,0:T(8,128)(2,1)}, u32[]{:S(2)}) copy-start(bf16[128,2048]{1,0:T(8,128)(2,1)} %param.13) | copy-start | bytes 1572868
  74.5 109.4 %all-gather.10.cloned.1.call-start = ((), (), s32[]{:S(2)}) async-start(), calls=%async_computation.5 | async-start | bytes 7208960 | tf_op jit(solution)/shard_map/all_gather | solution.py:87
  75.0 131.0 %all-gather.8.cloned.1.call-start = ((), (), s32[]{:S(2)}) async-start(), calls=%async_computation.4 | async-start | bytes 2621440 | tf_op jit(solution)/shard_map/all_gather | solution.py:84
  109.9 204.1 %all-gather.12.cloned.1.call-start = ((), (), s32[]{:S(2)}) async-start(), calls=%async_computation.6 | async-start | bytes 7208960 | tf_op jit(solution)/shard_map/all_gather | solution.py:92
  110.5 310.0 %all-gather.14.cloned.1.call-start = ((), (), s32[]{:S(2)}) async-start(), calls=%async_computation.7 | async-start | bytes 7208960 | tf_op jit(solution)/shard_map/all_gather | solution.py:96
  111.2 352.1 %reduce-scatter.5.cloned.1.call-start = ((), (), s32[]{:S(2)}) async-start(), calls=%async_computation.8 | async-start | bytes 2621440 | tf_op jit(solution)/shard_map/reduce_scatter | solution.py:97
  206.0 214.5 %copy-start.5 = (bf16[512,2048]{1,0:T(8,128)(2,1)S(1)}, bf16[512,2048]{1,0:T(8,128)(2,1)}, u32[]{:S(2)}) copy-start(bf16[512,2048]{1,0:T(8,128)(2,1)} %all-gather.8.cloned.1.call-done) | copy-start | bytes 6291460
  214.4 248.9 %copy-start.1 = (bf16[128,2048]{1,0:T(8,128)(2,1)S(1)}, bf16[128,2048]{1,0:T(8,128)(2,1)}, u32[]{:S(2)}) copy-start(bf16[128,2048]{1,0:T(8,128)(2,1)} %reduce-scatter.3.cloned.1.call-done) | copy-start | bytes 1572868
Sparse Core Ops, SparseCore 0:
  11.5 25.2 all-gather.5
  74.6 31.9 reduce-scatter.2
  433.8 29.4 reduce-scatter.4
Sparse Core Ops, SparseCore 1:
  76.5 107.3 all-gather.9
  185.3 20.7 all-gather.7
  207.5 106.5 all-gather.11
  315.6 104.8 all-gather.13
where the time goes:
time: 473 us
  waiting for transfers between devices  364 us (77%)
  blocking collectives  55.5 us (12%)
  matrix products  26.9 us (6%)
  between operations  14.9 us (3%)
  other arithmetic  11.5 us (2%)
    all_gather x1, waiting for transfers between devices, per_device(): lax.all_gather(ffn_down, 'fs', axis=0, tiled=True)  106 us
    all_gather x1, waiting for transfers between devices, per_device(): lax.all_gather(ffn_up, 'fs', axis=0, tiled=True)  99.6 us
    all_gather x1, waiting for transfers between devices, per_device(): lax.all_gather(ffn_gate, 'fs', axis=0, tiled=True)  72.6 us
    reduce_scatter x1, waiting for transfers between devices, per_device(): lax.psum_scatter(contract_last(gated_rows, out_rows).astype(jnp.bfloat16)...  31.4 us
    reduce_scatter x1, waiting for transfers between devices, per_device(): lax.psum_scatter(partial_value.astype(jnp.bfloat16), 'tp', scatter_dimens...  29.6 us
    all_gather x1, waiting for transfers between devices, per_device(): gathered = lax.all_gather(normed2, 'tp', axis=0, tiled=True)  22.1 us
    all_gather x1, blocking collectives, per_device(): lax.all_gather(gate_proj, 'fs', axis=0, tiled=True)  17.6 us
    all_gather x1, blocking collectives, per_device(): lax.all_gather(value_proj, 'fs', axis=0, tiled=True)  16.7 us
  transfers between devices with their start and end apart: 7, of which 6 were waited for; matrix products, arithmetic and copies ran while one was open for 3% of the time, Pallas kernels for 0%

commit v1 on v0

--- a/solution.py
+++ b/solution.py
@@ -1,9 +1,35 @@
+import functools
 import jax
 import jax.numpy as jnp
 from jax import lax
 from jax.sharding import PartitionSpec as P
 
 epsilon = 1e-06
+
+
+def pass_sources_all_on_mesh(xx, join_dim):
+    xx = jnp.moveaxis(xx, 0, join_dim)
+    z = xx.shape
+    return xx.reshape(*z[:join_dim], z[join_dim] * z[join_dim + 1], *z[join_dim + 2 :])
+
+
+def push_packet(z_in, group_axis):
+    wide_n = lax.axis_size(group_axis)
+    earlier = z_in[None]
+    for u in range(wide_n.bit_length() - 1):
+        back = 1 << u
+        res = lax.ppermute(earlier, group_axis, [(j0, j0 ^ back) for j0 in range(wide_n)])
+        step_out = jnp.stack([earlier, res])
+        after = lax.axis_index(group_axis) >> u & 1
+        earlier = jnp.where(after == 0, step_out, step_out[::-1]).reshape(-1, *z_in.shape)
+    return earlier
+
+
+def counts_mix(my_tile, body, axis_k):
+    return pass_sources_all_on_mesh(push_packet(my_tile, body), axis_k)
+
+
+search_heads = functools.partial(counts_mix, body="fs", axis_k=0)
 
 
 def rms_norm(rows, gain):
@@ -93,7 +119,7 @@
         preferred_element_type=jnp.float32,
     )
     hidden = (jax.nn.silu(gate_pre) * up_pre).astype(jnp.bfloat16)
-    partial_value = contract_last(hidden, lax.all_gather(ffn_down, "fs", axis=0, tiled=True))
+    partial_value = contract_last(hidden, search_heads(ffn_down))
     summed = lax.psum_scatter(
         partial_value.astype(jnp.bfloat16), "tp", scatter_dimension=0, tiled=True
     ).astype(jnp.float32)

time: 473 us -> 501 us (1.059)
  waiting for transfers between devices: 364 us -> 380 us
  other arithmetic: 11.5 us -> 20 us
    ppermute x0 -> x2, waiting for transfers between devices: none -> 317 us  [push_packet(): lax.ppermute(earlier, group_axis, [(j0, j0 ^ back) for j0 in range(wide_n)])]
    all_gather x1 -> x0, waiting for transfers between devices: 106 us -> none  [per_device(): lax.all_gather(ffn_down, 'fs', axis=0, tiled=True)]
    all_gather x1, waiting for transfers between devices: 99.6 us -> 0.01 us  [per_device(): lax.all_gather(ffn_up, 'fs', axis=0, tiled=True)]
    all_gather x1, waiting for transfers between devices: 72.6 us -> 0.01 us  [per_device(): lax.all_gather(ffn_gate, 'fs', axis=0, tiled=True)]
    all_gather x1, waiting for transfers between devices: 22.1 us -> 0.01 us  [per_device(): gathered = lax.all_gather(normed2, 'tp', axis=0, tiled=True)]
  transfers between devices with their start and end apart: 7 -> 8, of which waited for: 6 -> 4; matrix products, arithmetic and copies ran while one was open for 3% -> 4% of each run, Pallas kernels for 0% -> 0%
where the time goes in v1:
time: 501 us
  waiting for transfers between devices  380 us (76%)
  blocking collectives  55.5 us (11%)
  matrix products  26.9 us (5%)
  other arithmetic  20 us (4%)
  between operations  14.9 us (3%)
    ppermute x2, waiting for transfers between devices, push_packet(): lax.ppermute(earlier, group_axis, [(j0, j0 ^ back) for j0 in range(wide_n)])  317 us
    reduce_scatter x1, waiting for transfers between devices, per_device(): lax.psum_scatter(contract_last(gated_rows, out_rows).astype(jnp.bfloat16)...  31.4 us
    reduce_scatter x1, waiting for transfers between devices, per_device(): lax.psum_scatter(partial_value.astype(jnp.bfloat16), 'tp', scatter_dimens...  30.4 us
    all_gather x1, blocking collectives, per_device(): lax.all_gather(gate_proj, 'fs', axis=0, tiled=True)  17.6 us
    all_gather x1, blocking collectives, per_device(): lax.all_gather(value_proj, 'fs', axis=0, tiled=True)  16.7 us
    all_gather x1, blocking collectives, per_device(): lax.all_gather(out_proj, 'fs', axis=0, tiled=True)  15.6 us
    dot_general x2, matrix products, contract_last(): lax.dot_general(left, right, (((1,), (1,)), ((), ())), preferred_element_...  15.3 us
  transfers between devices with their start and end apart: 8, of which 4 were waited for; matrix products, arithmetic and copies ran while one was open for 4% of the time, Pallas kernels for 0%

profile of v1, /device:TPU:0, one launch (start us, length us, event | category | flops | bytes accessed | tf_op | source)
XLA Modules:
  0.0 500.6 jit_solution(4833336444624557414)
XLA Ops:
  7.4 0.7 convert_element_type.64
  8.1 1.2 fusion.3
  9.3 2.0 fusion.5
  11.5 0.7 bitcast_convert_fusion
  12.2 0.8 dynamic-slice_convert_fusion
  12.9 17.6 %all_gather.22 = bf16[2048,128]{1,0:T(8,128)(2,1)S(1)} all-gather(bf16[512,128]{1,0:T(8,128)(2,1)} %param.15), channel_id=1, replica_groups=mesh['rep'=2,'fs'=4,'tp'=4] {'fs'}, dimensions={0}, use_global_device_ids=true | all-gather | bytes 655360 | tf_op jit(solution)/shard_map/all_gather | solution.py:64
  30.5 16.7 %all_gather.23 = bf16[2048,128]{1,0:T(8,128)(2,1)S(1)} all-gather(bf16[512,128]{1,0:T(8,128)(2,1)S(1)} %copy-done.3), channel_id=1, replica_groups=mesh['rep'=2,'fs'=4,'tp'=4] {'fs'}, dimensions={0}, use_global_device_ids=true | all-gather | bytes 655360 | tf_op jit(solution)/shard_map/all_gather | solution.py:65
  47.2 15.6 %all_gather.24 = bf16[2048,128]{1,0:T(8,128)(2,1)S(1)} all-gather(bf16[512,128]{1,0:T(8,128)(2,1)S(1)} %copy-done.4), channel_id=1, replica_groups=mesh['rep'=2,'fs'=4,'tp'=4] {'fs'}, dimensions={0}, use_global_device_ids=true | all-gather | bytes 655360 | tf_op jit(solution)/shard_map/all_gather | solution.py:66
  62.8 2.3 fusion.11
  65.1 0.2 fusion.39
  65.4 5.7 %all-reduce = (f32[512]{0:T(512)S(1)}, f32[512]{0:T(512)S(1)}) all-reduce(f32[512]{0:T(512)S(1)} %get-tuple-element.6, f32[512]{0:T(512)S(1)} %get-tuple-element.5), channel_id=1, replica_groups=mesh['rep'=2,'fs'=4,'tp'=4] {'tp'}, use_global_device_ids=true, to_apply=%region_4.5 | all-reduce | flops 1024 | bytes 8192 | tf_op jit(solution)/shard_map/psum | solution.py:81
  71.1 0.2 add_convert_fusion
  71.3 0.9 convolution_add_fusion
  72.4 2.0 convolution_convert_fusion
  74.5 0.5 all-gather.9.cloned.1.call-update
  75.1 31.4 %reduce-scatter.3.cloned.1.call-done = bf16[128,2048]{1,0:T(8,128)(2,1)} async-done(((bf16[512,2048]{1,0:T(8,128)(2,1)}), bf16[128,2048]{1,0:T(8,128)(2,1)}) %reduce-scatter.3.cloned.1.call-update) | async-done | bytes 524304 | tf_op jit(solution)/shard_map/reduce_scatter | solution.py:102
  106.5 1.3 fusion.7
  107.8 2.0 fusion.9
  110.0 0.5 all-gather.11.cloned.1.call-update
  110.5 0.2 reduce-scatter.5.cloned.1.call-start
  110.7 1.6 collective-permute-start
  112.3 98.4 %collective-permute-done = bf16[1,512,1408]{2,1,0:T(8,128)(2,1)S(1)} collective-permute-done((bf16[1,512,1408]{2,1,0:T(8,128)(2,1)S(1)}, bf16[1,512,1408]{2,1,0:T(8,128)(2,1)S(1)}, u32[]{:S(2)}, u32[]{:S(2)}) %collective-permute-start) | collective-permute-done | bytes 1441824 | tf_op jit(solution)/shard_map/ppermute | solution.py:21
  210.6 0.3 pad_maximum_fusion.1
  210.9 2.2 fusion.2
  213.2 1.0 collective-permute-start.1
  214.1 218.9 %collective-permute-done.1 = bf16[2,512,1408]{2,1,0:T(8,128)(2,1)} collective-permute-done((bf16[2,512,1408]{2,1,0:T(8,128)(2,1)}, bf16[2,512,1408]{2,1,0:T(8,128)(2,1)}, u32[]{:S(2)}, u32[]{:S(2)}) %collective-permute-start.1) | collective-permute-done | bytes 2883616 | tf_op jit(solution)/shard_map/ppermute | solution.py:21
  433.0 2.4 pad_maximum_fusion
  435.4 3.6 reverse_select_fusion
  439.1 8.4 %fusion.40 = f32[512,1408]{1,0:T(8,128)} fusion(bf16[512,2048]{1,0:T(8,128)(2,1)} %all-gather.7.cloned.1.call-done, bf16[2048,1408]{1,0:T(8,128)(2,1)} %all-gather.9.cloned.1.call-done), kind=kOutput, calls=%fused_computation.66 | convolution fusion | flops 2952790016 | bytes 10747904 | tf_op jit(solution)/shard_map/dot_general | solution.py:111
  447.5 13.3 %convolution_convert_fusion.1 = bf16[512,2048]{1,0:T(8,128)(2,1)} fusion(bf16[2048,1408]{1,0:T(8,128)(2,1)} %bitcast.30, bf16[512,2048]{1,0:T(8,128)(2,1)S(1)} %copy-done.6, bf16[2048,1408]{1,0:T(8,128)(2,1)} %all-gather.11.cloned.1.call-done, f32[512,1408]{1,0:T(8,128)} %fusion.40), kind=kOutput, calls=%fused_computation.6 | convolution fusion | flops 5910953984 | bytes 18612224 | tf_op jit(solution)/shard_map/dot_general | solution.py:42
  460.8 30.4 %reduce-scatter.5.cloned.1.call-done = bf16[128,2048]{1,0:T(8,128)(2,1)} async-done(((bf16[512,2048]{1,0:T(8,128)(2,1)}), bf16[128,2048]{1,0:T(8,128)(2,1)}) %reduce-scatter.5.cloned.1.call-update) | async-done | bytes 524304 | tf_op jit(solution)/shard_map/reduce_scatter | solution.py:123
  491.2 2.1 fusion.10
  (33 shorter events, 0.4 us)
Async XLA Ops:
  7.4 23.2 %copy-start.3 = (bf16[512,128]{1,0:T(8,128)(2,1)S(1)}, bf16[512,128]{1,0:T(8,128)(2,1)}, u32[]{:S(2)}) copy-start(bf16[512,128]{1,0:T(8,128)(2,1)} %param.16) | copy-start | bytes 393220
  7.4 39.9 %copy-start.4 = (bf16[512,128]{1,0:T(8,128)(2,1)S(1)}, bf16[512,128]{1,0:T(8,128)(2,1)}, u32[]{:S(2)}) copy-start(bf16[512,128]{1,0:T(8,128)(2,1)} %param.21) | copy-start | bytes 393220
  7.4 55.5 %all-gather.5.cloned.1.call-start = ((), (), s32[]{:S(2)}) async-start(), calls=%async_computation.2 | async-start | bytes 2621440 | tf_op jit(solution)/shard_map/all_gather | solution.py:77
  11.4 95.1 %reduce-scatter.3.cloned.1.call-start = ((), (), s32[]{:S(2)}) async-start(), calls=%async_computation.3 | async-start | bytes 2621440 | tf_op jit(solution)/shard_map/reduce_scatter | solution.py:102
  72.3 2.7 copy-start.5
  72.3 34.2 %copy-start = (bf16[128,2048]{1,0:T(8,128)(2,1)S(1)}, bf16[128,2048]{1,0:T(8,128)(2,1)}, u32[]{:S(2)}) copy-start(bf16[128,2048]{1,0:T(8,128)(2,1)} %param.13) | copy-start | bytes 1572868
  74.4 36.3 %copy-start.2 = (bf16[512,1408]{1,0:T(8,128)(2,1)S(1)}, bf16[512,1408]{1,0:T(8,128)(2,1)}, u32[]{:S(2)}) copy-start(bf16[512,1408]{1,0:T(8,128)(2,1)} %param.25) | copy-start | bytes 4325380
  74.4 364.7 %all-gather.9.cloned.1.call-start = ((), (), s32[]{:S(2)}) async-start(), calls=%async_computation.5 | async-start | bytes 7208960 | tf_op jit(solution)/shard_map/all_gather | solution.py:113
  75.0 364.1 %all-gather.7.cloned.1.call-start = ((), (), s32[]{:S(2)}) async-start(), calls=%async_computation.4 | async-start | bytes 2621440 | tf_op jit(solution)/shard_map/all_gather | solution.py:110
  109.9 337.6 %all-gather.11.cloned.1.call-start = ((), (), s32[]{:S(2)}) async-start(), calls=%async_computation.6 | async-start | bytes 7208960 | tf_op jit(solution)/shard_map/all_gather | solution.py:118
  110.5 380.7 %reduce-scatter.5.cloned.1.call-start = ((), (), s32[]{:S(2)}) async-start(), calls=%async_computation.7 | async-start | bytes 2621440 | tf_op jit(solution)/shard_map/reduce_scatter | solution.py:123
  110.7 99.9 %collective-permute-start = (bf16[1,512,1408]{2,1,0:T(8,128)(2,1)S(1)}, bf16[1,512,1408]{2,1,0:T(8,128)(2,1)S(1)}, u32[]{:S(2)}, u32[]{:S(2)}) collective-permute-start(bf16[1,512,1408]{2,1,0:T(8,128)(2,1)S(1)} %bitcast.31), channel_id=1, source_target_pairs={{0,4},{4,0},{8,12},{12,8},{1,5},{5,1},{9,13},{13,9},{2,6},{6,2},{1... | collective-permute-start | bytes 4325384 | tf_op jit(solution)/shard_map/ppermute | solution.py:21
  213.2 219.9 %collective-permute-start.1 = (bf16[2,512,1408]{2,1,0:T(8,128)(2,1)}, bf16[2,512,1408]{2,1,0:T(8,128)(2,1)}, u32[]{:S(2)}, u32[]{:S(2)}) collective-permute-start(bf16[2,512,1408]{2,1,0:T(8,128)(2,1)} %get-tuple-element.10), channel_id=1, source_target_pairs={{0,8},{4,12},{8,0},{12,4},{1,9},{5,13},{9,1},{13,5},{2,10},{6,14},... | collective-permute-start | bytes 8650760 | tf_op jit(solution)/shard_map/ppermute | solution.py:21
  439.1 8.4 %copy-start.6 = (bf16[512,2048]{1,0:T(8,128)(2,1)S(1)}, bf16[512,2048]{1,0:T(8,128)(2,1)}, u32[]{:S(2)}) copy-start(bf16[512,2048]{1,0:T(8,128)(2,1)} %all-gather.7.cloned.1.call-done) | copy-start | bytes 6291460
  447.5 43.7 %copy-start.1 = (bf16[128,2048]{1,0:T(8,128)(2,1)S(1)}, bf16[128,2048]{1,0:T(8,128)(2,1)}, u32[]{:S(2)}) copy-start(bf16[128,2048]{1,0:T(8,128)(2,1)} %reduce-scatter.3.cloned.1.call-done) | copy-start | bytes 1572868
Sparse Core Ops, SparseCore 0:
  11.5 25.2 all-gather.4
  74.5 31.9 reduce-scatter.2
  460.9 30.2 reduce-scatter.4
Sparse Core Ops, SparseCore 1:
  76.5 136.0 all-gather.8
  213.9 22.5 all-gather.6
  238.0 179.8 all-gather.10
